TPU v7x, 512 devices: a whole 4x8x8 slice. The times are simulated.
512 devices in a mesh: sp: 64 (over z, y), tp: 8 (over x, core).
Axes of the slice: x: 4, y: 8, z: 8, core: 2. Of those that a mesh axis runs over, the one named last changes fastest.
Arguments:
- resid: bfloat16 [32768, 2048], P(('sp', 'tp')), may hold values from -3 to 3
- queries: bfloat16 [32768, 1024], P('sp', 'tp'), may hold values from -6 to 6
- keys: bfloat16 [32768, 512], P('sp', 'tp'), may hold values from -6 to 6
- values: bfloat16 [32768, 512], P('sp', 'tp'), may hold values from -6 to 6
- documents: int32 [32768], P('sp'), may hold values from 0 to 31, never falling along the last dimension, each value on 1 to 2048 neighbouring positions
- sinks: float32 [16], P('tp'), may hold values from 0 to 5
- out_proj: bfloat16 [1024, 2048], replicated, may hold values from -0.75 to 0.75
- norm_gain: float32 [2048], replicated, may hold values from 0.1 to 1.9
- gate_proj: bfloat16 [2048, 5632], P('sp', 'tp'), may hold values from -0.125 to 0.125
- up_proj: bfloat16 [2048, 5632], P('sp', 'tp'), may hold values from -0.125 to 0.125
- down_proj: bfloat16 [5632, 2048], P('tp', 'sp'), may hold values from -0.078125 to 0.078125
Outputs:
- mixed: bfloat16 [32768, 2048], P(('sp', 'tp'))
Inputs may be any that keep to these rules, and one draw needn't show every extreme that they name: `documents`: document numbers never fall along the sequence; each document holds at most 2048 positions.
All inputs are finite; a program needn't handle non-finite values.
Results may differ from a plain program's by a relative error of at most 0.0095.
Values may be sent and summed in bfloat16 or wider, within the bound.
A program may use at most 64 MiB of HBM per device.

v0:
```python
import jax
import jax.numpy as jnp
from jax import lax
from jax.sharding import PartitionSpec as P

HD = 64
WINDOW = 128


def passed_along(value, axis, steps):
    count = lax.axis_size(axis)
    first, last = (max(0, -steps), min(count, count - steps))
    return lax.ppermute(value, axis, [(source, source + steps) for source in range(first, last)])


def rows_first(arrays, axis, dims):
    turned = [jnp.moveaxis(a, dim, 0) for a, dim in zip(arrays, dims)]
    widths = [t[0].size for t in turned]
    both = jnp.concatenate([t.reshape(-1, w) for t, w in zip(turned, widths)], axis=1)
    whole = lax.all_gather(both, axis, axis=0, tiled=True)
    tiles = jnp.split(whole, [sum(widths[:k]) for k in range(1, len(widths))], axis=1)
    return tuple(
        (
            jnp.moveaxis(b.reshape(-1, *t.shape[1:]), 0, dim)
            for b, t, dim in zip(tiles, turned, dims)
        )
    )


def in_order(tiles, dim):
    dims = list(tiles.shape[1:])
    dims[dim] *= tiles.shape[0]
    return jnp.moveaxis(tiles, 0, dim).reshape(dims)


def from_everyone(x, axis):
    size = lax.axis_size(axis)
    return lax.all_to_all(jnp.broadcast_to(x[None], (size, *x.shape)), axis, 0, 0, tiled=True)


def gather_directly(x, axis, dim):
    return in_order(from_everyone(x, axis), dim)


def in_blocks(x, dim, size):
    before, after = (x.shape[:dim], x.shape[dim + 1 :])
    return jnp.moveaxis(x.reshape(*before, size, -1, *after), dim, 0)


def sum_at_owner(x, axis, dim):
    size = lax.axis_size(axis)
    tiles = lax.all_to_all(in_blocks(x, dim, size), axis, 0, 0, tiled=True)
    return jnp.sum(tiles.astype(jnp.float32), axis=0)


def attend(queries, keys, values, documents, sinks):
    rows = queries.shape[0]
    kv_heads = keys.shape[1] // HD
    group = queries.shape[1] // HD // kv_heads
    blocks = rows // WINDOW
    key_value = jnp.concatenate([keys, values], axis=1)
    tail_pair, tail_docs = passed_along(
        (key_value[rows - WINDOW :], documents[rows - WINDOW :].astype(jnp.bfloat16)), "sp", 1
    )
    ext_pair = jnp.concatenate([tail_pair, key_value], axis=0).reshape(
        blocks + 1, WINDOW, 2 * kv_heads * HD
    )
    ext_docs = jnp.concatenate([tail_docs.astype(jnp.int32), documents], axis=0).reshape(
        blocks + 1, WINDOW
    )
    band = jnp.concatenate([ext_pair[:-1], ext_pair[1:]], axis=1)
    band_keys = band[:, :, : kv_heads * HD].reshape(blocks, 2 * WINDOW, kv_heads, HD)
    band_values = band[:, :, kv_heads * HD :].reshape(blocks, 2 * WINDOW, kv_heads, HD)
    band_docs = jnp.concatenate([ext_docs[:-1], ext_docs[1:]], axis=1)
    query_docs = documents.reshape(blocks, WINDOW)
    offset = lax.axis_index("sp") * rows
    distance = jnp.arange(WINDOW)[:, None] + WINDOW - jnp.arange(2 * WINDOW)[None, :]
    key_pos = (
        offset + jnp.arange(blocks)[:, None] * WINDOW + jnp.arange(2 * WINDOW)[None, :] - WINDOW
    )
    visible = (
        ((distance >= 0) & (distance < WINDOW))[None]
        & (key_pos >= 0)[:, None, :]
        & (band_docs[:, None, :] == query_docs[:, :, None])
    )
    query_blocks = queries.reshape(blocks, WINDOW, kv_heads, group, HD)
    scores = jnp.einsum(
        "nikgd,njkd->nkgij", query_blocks, band_keys, preferred_element_type=jnp.float32
    ) * HD ** (-0.5)
    scores = jnp.where(visible[:, None, None], scores, -jnp.inf)
    sink_logit = sinks.reshape(kv_heads, group)[None, :, :, None, None]
    row_top = jnp.maximum(jnp.max(scores, axis=-1, keepdims=True), sink_logit)
    raw_weights = jnp.exp(scores - row_top)
    totals = jnp.sum(raw_weights, axis=-1, keepdims=True) + jnp.exp(sink_logit - row_top)
    weights = (raw_weights / totals).astype(jnp.bfloat16)
    attended = jnp.einsum(
        "nkgij,njkd->nikgd", weights, band_values, preferred_element_type=jnp.float32
    )
    return attended.astype(jnp.bfloat16).reshape(rows, kv_heads * group * HD)


def norm_rows(mid_rows, norm_gain):
    scale = lax.rsqrt(jnp.mean(mid_rows * mid_rows, axis=-1, keepdims=True) + 1e-06)
    return (mid_rows * scale * norm_gain).astype(jnp.bfloat16)


def shards(
    resid,
    queries,
    keys,
    values,
    documents,
    sinks,
    out_proj,
    norm_gain,
    gate_proj,
    up_proj,
    down_proj,
):
    gate_whole, up_whole, down_whole = rows_first((gate_proj, up_proj, down_proj), "sp", (0, 0, 1))
    attended = attend(queries, keys, values, documents, sinks)
    own_heads = lax.all_to_all(attended, "tp", split_axis=0, concat_axis=1, tiled=True)
    mid_rows = resid.astype(jnp.float32) + jnp.dot(
        own_heads, out_proj, preferred_element_type=jnp.float32
    )
    normed = gather_directly(norm_rows(mid_rows, norm_gain), "tp", 0)
    gate_acts = jnp.dot(normed, gate_whole, preferred_element_type=jnp.float32)
    up_acts = jnp.dot(normed, up_whole, preferred_element_type=jnp.float32)
    hidden = (jax.nn.silu(gate_acts) * up_acts).astype(jnp.bfloat16)
    summed = sum_at_owner(
        jnp.dot(hidden, down_whole, preferred_element_type=jnp.float32).astype(jnp.bfloat16),
        "tp",
        0,
    )
    return (mid_rows + summed).astype(jnp.bfloat16)


def solution(mesh):
    in_specs = (
        P(("sp", "tp"), None),
        P("sp", "tp"),
        P("sp", "tp"),
        P("sp", "tp"),
        P("sp"),
        P("tp"),
        P(),
        P(),
        P("sp", "tp"),
        P("sp", "tp"),
        P("tp", "sp"),
    )
    out_specs = P(("sp", "tp"), None)
    return jax.shard_map(shards, mesh=mesh, in_specs=in_specs, out_specs=out_specs, check_vma=False)
```

profile of v0, /device:TPU:1, one launch (start us, length us, event | category | flops | bytes accessed | tf_op | source)
XLA Modules:
  0.0 170.7 jit_solution(16067916554664489220)
XLA Ops:
  6.5 1.6 concatenate.23
  8.2 0.7 convert.3
  8.9 4.0 %collective-permute-start.1 = (bf16[128]{0:T(256)(128)(2,1)S(1)}, bf16[128]{0:T(256)(128)(2,1)S(1)}, u32[]{:S(2)}, u32[]{:S(2)}) collective-permute-start(bf16[128]{0:T(256)(128)(2,1)S(1)} %slice.48), channel_id=1, source_target_pairs={{0,8},{8,16},{16,24},{24,32},{32,40},{40,48},{48,56},{56,64},{64,7... | collective-permute-start | bytes 776 | tf_op jit(solution)/shard_map/ppermute | solution.py:13
  12.9 1.0 copy.23
  13.9 1.0 copy.24
  14.8 0.1 fusion.35
  14.9 3.2 %collective-permute-start = (bf16[128,128]{1,0:T(8,128)(2,1)S(1)}, bf16[128,128]{1,0:T(8,128)(2,1)S(1)}, u32[]{:S(2)}, u32[]{:S(2)}) collective-permute-start(bf16[128,128]{1,0:T(8,128)(2,1)S(1)} %fusion.35), channel_id=1, source_target_pairs={{0,8},{8,16},{16,24},{24,32},{32,40},{40,48},{48,56},{56,64},{64,7... | collective-permute-start | bytes 98312 | tf_op jit(solution)/shard_map/ppermute | solution.py:13
  18.2 0.1 add_compare_fusion
  18.3 1.0 reshape.150
  19.4 0.7 pad_add_fusion
  20.1 0.7 pad_add_fusion.1
  20.7 1.0 compare_and_fusion
  21.8 0.1 pad_maximum_fusion.1
  21.9 0.1 copy.25
  22.1 0.1 copy.26
  22.2 0.4 fusion.39
  22.6 0.2 fusion.20
  22.8 0.1 exponential_add_fusion
  22.9 0.3 fusion.19
  23.2 0.2 copy.38
  23.4 0.1 reshape.151
  23.5 10.6 %all_to_all.29 = bf16[8,64,128]{2,1,0:T(8,128)(2,1)S(1)} all-to-all(bf16[8,64,128]{2,1,0:T(8,128)(2,1)S(1)} %reshape.151), channel_id=1, replica_groups=mesh['sp'=64,'tp'=8] {'tp'}, dimensions={0} | all-to-all | bytes 262144 | tf_op jit(solution)/shard_map/all_to_all | solution.py:122
  34.1 3.2 %multiply_reduce_fusion = (f32[64]{0:T(128)S(1)}, f32[64,2048]{1,0:T(8,128)S(1)}) fusion(bf16[1024,2048]{1,0:T(8,128)(2,1)} %param.17, bf16[64,2048]{1,0:T(8,128)(2,1)S(1)} %copy-done, bf16[8,64,128]{2,1,0:T(8,128)(2,1)S(1)} %all_to_all.29), kind=kOutput, calls=%fused_computation.23 | convolution fusion | flops 268959680 | bytes 5112064 | tf_op jit(solution)/shard_map/dot_general | solution.py:123
  37.3 0.1 multiply_convert_fusion
  37.5 0.2 broadcast_in_dim.16
  37.7 29.5 %all_to_all.30 = bf16[8,64,2048]{2,1,0:T(8,128)(2,1)S(1)} all-to-all(bf16[8,64,2048]{2,1,0:T(8,128)(2,1)S(1)} %broadcast_in_dim.16), channel_id=1, replica_groups=mesh['sp'=64,'tp'=8] {'tp'}, dimensions={0} | all-to-all | bytes 4194304 | tf_op jit(solution)/shard_map/all_to_all | solution.py:38
  67.2 50.1 %all-gather.2.cloned.1.call-done = bf16[2048,2112]{1,0:T(8,128)(2,1)} async-done(((bf16[32,2112]{1,0:T(8,128)(2,1)}), bf16[2048,2112]{1,0:T(8,128)(2,1)}) %all-gather.2.cloned.1.call-update) | async-done | bytes 8650768 | tf_op jit(solution)/shard_map/all_gather | solution.py:20
  117.3 4.7 %fusion.4 = f32[512,704]{0,1:T(8,128)} fusion(bf16[512,2048]{1,0:T(8,128)(2,1)S(1)} %bitcast.48, bf16[2048,2112]{1,0:T(8,128)(2,1)} %all-gather.2.cloned.1.call-done), kind=kOutput, calls=%fused_computation.5 | convolution fusion | flops 1476395008 | bytes 6684672 | tf_op jit(solution)/shard_map/dot_general | solution.py:127
  121.9 9.5 %fusion.6 = bf16[512,2048]{1,0:T(8,128)(2,1)} fusion(bf16[2048,2112]{1,0:T(8,128)(2,1)} %all-gather.2.cloned.1.call-done, bf16[512,2048]{1,0:T(8,128)(2,1)S(1)} %bitcast.49, f32[512,704]{0,1:T(8,128)} %fusion.4), kind=kOutput, calls=%fused_computation.7 | convolution fusion | flops 2956001280 | bytes 11927552 | tf_op jit(solution)/shard_map/dot_general | solution.py:131
  131.4 31.3 %all_to_all.31 = bf16[8,64,2048]{2,1,0:T(8,128)(2,1)S(1)} all-to-all(bf16[8,64,2048]{2,1,0:T(8,128)(2,1)} %bitcast.50), channel_id=1, replica_groups=mesh['sp'=64,'tp'=8] {'tp'}, dimensions={0} | all-to-all | bytes 4194304 | tf_op jit(solution)/shard_map/all_to_all | solution.py:52
  162.7 0.4 convert_reduce_fusion
  163.1 0.8 add_convert_fusion
  (18 shorter events, 0.2 us)
Async XLA Ops:
  6.5 110.7 %all-gather.2.cloned.1.call-start = ((), (), s32[]{:S(2)}) async-start(), calls=%async_computation.3 | async-start | bytes 9052160 | tf_op jit(solution)/shard_map/all_gather | solution.py:20
  8.2 14.4 %copy-start.2 = (f32[2]{0:T(128)S(1)}, f32[2]{0:T(128)}, u32[]{:S(2)}) copy-start(f32[2]{0:T(128)} %param.16) | copy-start | bytes 28
  8.9 10.5 %collective-permute-start.1 = (bf16[128]{0:T(256)(128)(2,1)S(1)}, bf16[128]{0:T(256)(128)(2,1)S(1)}, u32[]{:S(2)}, u32[]{:S(2)}) collective-permute-start(bf16[128]{0:T(256)(128)(2,1)S(1)} %slice.48), channel_id=1, source_target_pairs={{0,8},{8,16},{16,24},{24,32},{32,40},{40,48},{48,56},{56,64},{64,7... | collective-permute-start | bytes 776 | tf_op jit(solution)/shard_map/ppermute | solution.py:13
  14.9 6.8 %collective-permute-start = (bf16[128,128]{1,0:T(8,128)(2,1)S(1)}, bf16[128,128]{1,0:T(8,128)(2,1)S(1)}, u32[]{:S(2)}, u32[]{:S(2)}) collective-permute-start(bf16[128,128]{1,0:T(8,128)(2,1)S(1)} %fusion.35), channel_id=1, source_target_pairs={{0,8},{8,16},{16,24},{24,32},{32,40},{40,48},{48,56},{56,64},{64,7... | collective-permute-start | bytes 98312 | tf_op jit(solution)/shard_map/ppermute | solution.py:13
  22.9 11.2 %copy-start = (bf16[64,2048]{1,0:T(8,128)(2,1)S(1)}, bf16[64,2048]{1,0:T(8,128)(2,1)}, u32[]{:S(2)}) copy-start(bf16[64,2048]{1,0:T(8,128)(2,1)} %param.11) | copy-start | bytes 786436
  34.1 3.2 %copy-start.1 = (f32[2048]{0:T(1024)S(1)}, f32[2048]{0:T(1024)}, u32[]{:S(2)}) copy-start(f32[2048]{0:T(1024)} %param.18) | copy-start | bytes 24580
Sparse Core Ops, SparseCore 0:
  10.3 106.8 all-gather.1
where the time goes:
time: 171 us
  blocking collectives  71.3 us (42%)
  waiting for transfers between devices  50.1 us (29%)
  matrix products  18 us (11%)
  between operations  13.6 us (8%)
  starting transfers between devices  7.21 us (4%)
  local copies, waits for them, and re-layouts  5.42 us (3%)
  other arithmetic  5 us (3%)
    all_gather x1, waiting for transfers between devices, rows_first(): whole = lax.all_gather(both, axis, axis=0, tiled=True)  50.1 us
    all_to_all x1, blocking collectives, sum_at_owner(): tiles = lax.all_to_all(in_blocks(x, dim, size), axis, 0, 0, tiled=True)  31.3 us
    all_to_all x1, blocking collectives, from_everyone(): lax.all_to_all(jnp.broadcast_to(x[None], (size, *x.shape)), axis, 0, 0, t...  29.5 us
    all_to_all x1, blocking collectives, shards(): lax.all_to_all(attended, 'tp', split_axis=0, concat_axis=1, tiled=True)  10.6 us
    dot_general x1, matrix products, shards(): jnp.dot(hidden, down_whole, preferred_element_type=jnp.float32)  9.48 us
    ppermute x2, starting transfers between devices, passed_along(): lax.ppermute(value, axis, [(source, source + steps) for source in range(f...  7.21 us
    dot_general x1, matrix products, shards(): gate_acts = jnp.dot(normed, gate_whole, preferred_element_type=jnp.float32)  4.67 us
  transfers between devices with their start and end apart: 3, of which 1 were waited for; matrix products, arithmetic and copies ran while one was open for 7% of the time, Pallas kernels for 0%

commit v1 on v0

--- a/solution.py
+++ b/solution.py
@@ -5,6 +5,11 @@
 
 HD = 64
 WINDOW = 128
+
+
+def exchange_gather(x, axis, dim):
+    sent = jnp.stack([x] * lax.axis_size(axis))
+    return jnp.concatenate(lax.all_to_all(sent, axis, 0, 0), axis=dim)
 
 
 def passed_along(value, axis, steps):
@@ -17,7 +22,7 @@
     turned = [jnp.moveaxis(a, dim, 0) for a, dim in zip(arrays, dims)]
     widths = [t[0].size for t in turned]
     both = jnp.concatenate([t.reshape(-1, w) for t, w in zip(turned, widths)], axis=1)
-    whole = lax.all_gather(both, axis, axis=0, tiled=True)
+    whole = exchange_gather(both, axis, 0)
     tiles = jnp.split(whole, [sum(widths[:k]) for k in range(1, len(widths))], axis=1)
     return tuple(
         (

time: 171 us -> 342 us (2.00)
  the two profiles are of different devices: /device:TPU:1 before, /device:TPU:24 now
where the time goes in v1:
time: 342 us
  blocking collectives  271 us (79%)
  waiting for transfers between devices  28.6 us (8%)
  matrix products  16.2 us (5%)
  starting transfers between devices  11 us (3%)
  local copies, waits for them, and re-layouts  9.33 us (3%)
  other arithmetic  4.98 us (1%)
    all_to_all x1, blocking collectives, exchange_gather(): return jnp.concatenate(lax.all_to_all(sent, axis, 0, 0), axis=dim)  231 us
    all_to_all x1, blocking collectives, sum_at_owner(): tiles = lax.all_to_all(in_blocks(x, dim, size), axis, 0, 0, tiled=True)  30.7 us
    all_to_all x1, waiting for transfers between devices, from_everyone(): lax.all_to_all(jnp.broadcast_to(x[None], (size, *x.shape)), axis, 0, 0, t...  27 us
    all_to_all x1, blocking collectives, shards(): lax.all_to_all(attended, 'tp', split_axis=0, concat_axis=1, tiled=True)  10.2 us
    dot_general x1, matrix products, shards(): jnp.dot(hidden, down_whole, preferred_element_type=jnp.float32)  9.5 us
    ppermute x2, starting transfers between devices, passed_along(): lax.ppermute(value, axis, [(source, source + steps) for source in range(f...  7.27 us
  transfers between devices with their start and end apart: 3, of which 2 were waited for; matrix products, arithmetic and copies ran while one was open for 1% of the time, Pallas kernels for 0%

profile of v1, /device:TPU:24, one launch (start us, length us, event | category | flops | bytes accessed | tf_op | source)
XLA Modules:
  0.0 341.8 jit_solution(11323738596201779134)
XLA Ops:
  0.0 1.0 copy.23
  1.0 1.0 copy.24
  2.0 4.7 %collective-permute-start = (bf16[128,128]{1,0:T(8,128)(2,1)S(1)}, bf16[128,128]{1,0:T(8,128)(2,1)S(1)}, u32[]{:S(2)}, u32[]{:S(2)}) collective-permute-start(bf16[128,128]{1,0:T(8,128)(2,1)S(1)} %fusion.35), channel_id=1, source_target_pairs={{0,8},{8,16},{16,24},{24,32},{32,40},{40,48},{48,56},{56,64},{64,7... | collective-permute-start | bytes 98312 | tf_op jit(solution)/shard_map/ppermute | solution.py:18
  6.7 0.7 convert.3
  7.4 2.6 collective-permute-start.1
  10.2 1.0 reshape.156
  11.2 1.7 collective-permute-done.1
  12.9 0.7 pad_add_fusion
  13.6 0.7 pad_add_fusion.1
  14.3 1.0 compare_and_fusion
  15.3 0.1 pad_maximum_fusion.1
  15.4 0.1 copy.26
  15.6 0.1 copy.25
  15.7 0.4 fusion.39
  16.2 0.2 fusion.20
  16.4 0.3 fusion.19
  16.7 0.2 copy.38
  16.9 0.1 reshape.157
  17.1 10.2 %all_to_all.34 = bf16[8,64,128]{2,1,0:T(8,128)(2,1)S(1)} all-to-all(bf16[8,64,128]{2,1,0:T(8,128)(2,1)S(1)} %reshape.157), channel_id=1, replica_groups=mesh['sp'=64,'tp'=8] {'tp'}, dimensions={0} | all-to-all | bytes 262144 | tf_op jit(solution)/shard_map/all_to_all | solution.py:127
  27.3 3.2 multiply_reduce_fusion
  30.5 0.1 multiply_convert_fusion
  30.6 1.6 broadcast_in_dim.16
  32.2 3.7 %all-to-all-start.1 = ((bf16[8,64,2048]{2,1,0:T(8,128)(2,1)}), bf16[8,64,2048]{2,1,0:T(8,128)(2,1)S(1)}, u32[]{:S(2)}, u32[]{:S(2)}) async-start(bf16[8,64,2048]{2,1,0:T(8,128)(2,1)} %broadcast_in_dim.16), calls=%async_computation.1 | async-start | bytes 4194304 | tf_op jit(solution)/shard_map/all_to_all | solution.py:43
  36.1 27.0 %all-to-all-done.1 = bf16[8,64,2048]{2,1,0:T(8,128)(2,1)S(1)} async-done(((bf16[8,64,2048]{2,1,0:T(8,128)(2,1)}), bf16[8,64,2048]{2,1,0:T(8,128)(2,1)S(1)}, u32[]{:S(2)}, u32[]{:S(2)}) %all-to-all-start.1) | async-done | bytes 2097184 | tf_op jit(solution)/shard_map/all_to_all | solution.py:43
  63.1 0.6 stack.2
  63.7 230.5 %all_to_all.35 = bf16[64,32,2112]{2,1,0:T(8,128)(2,1)S(1)} all-to-all(bf16[64,32,2112]{2,1,0:T(8,128)(2,1)S(1)} %stack.2), channel_id=1, replica_groups=mesh['sp'=64,'tp'=8] {'sp'}, dimensions={0} | all-to-all | bytes 17301504 | tf_op jit(solution)/shard_map/all_to_all | solution.py:12
  294.2 3.4 %copy-done = bf16[64,32,2112]{2,1,0:T(8,128)(2,1)} copy-done((bf16[64,32,2112]{2,1,0:T(8,128)(2,1)}, bf16[64,32,2112]{2,1,0:T(8,128)(2,1)S(1)}, u32[]{:S(2)}) %copy-start) | copy-done | bytes 8650776
  297.6 2.8 fusion.4
  300.4 9.5 %fusion.6 = bf16[512,2048]{1,0:T(8,128)(2,1)} fusion(bf16[2048,2112]{1,0:T(8,128)(2,1)} %bitcast.50, bf16[512,2048]{1,0:T(8,128)(2,1)S(1)} %bitcast.52, f32[512,704]{0,1:T(8,128)} %fusion.4), kind=kOutput, calls=%fused_computation.7 | convolution fusion | flops 2956001280 | bytes 11927552 | tf_op jit(solution)/shard_map/dot_general | solution.py:136
  309.9 30.7 %all_to_all.36 = bf16[8,64,2048]{2,1,0:T(8,128)(2,1)S(1)} all-to-all(bf16[8,64,2048]{2,1,0:T(8,128)(2,1)} %bitcast.53), channel_id=1, replica_groups=mesh['sp'=64,'tp'=8] {'tp'}, dimensions={0} | all-to-all | bytes 4194304 | tf_op jit(solution)/shard_map/all_to_all | solution.py:57
  340.6 0.3 convert_reduce_fusion
  341.0 0.8 add_convert_fusion
  (26 shorter events, 0.5 us)
Async XLA Ops:
  0.0 16.1 %copy-start.6 = (f32[2]{0:T(128)S(1)}, f32[2]{0:T(128)}, u32[]{:S(2)}) copy-start(f32[2]{0:T(128)} %param.16) | copy-start | bytes 28
  2.0 13.3 %collective-permute-start = (bf16[128,128]{1,0:T(8,128)(2,1)S(1)}, bf16[128,128]{1,0:T(8,128)(2,1)S(1)}, u32[]{:S(2)}, u32[]{:S(2)}) collective-permute-start(bf16[128,128]{1,0:T(8,128)(2,1)S(1)} %fusion.35), channel_id=1, source_target_pairs={{0,8},{8,16},{16,24},{24,32},{32,40},{40,48},{48,56},{56,64},{64,7... | collective-permute-start | bytes 98312 | tf_op jit(solution)/shard_map/ppermute | solution.py:18
  7.4 5.5 %collective-permute-start.1 = (bf16[128]{0:T(256)(128)(2,1)S(1)}, bf16[128]{0:T(256)(128)(2,1)S(1)}, u32[]{:S(2)}, u32[]{:S(2)}) collective-permute-start(bf16[128]{0:T(256)(128)(2,1)S(1)} %slice.48), channel_id=1, source_target_pairs={{0,8},{8,16},{16,24},{24,32},{32,40},{40,48},{48,56},{56,64},{64,7... | collective-permute-start | bytes 776 | tf_op jit(solution)/shard_map/ppermute | solution.py:18
  16.4 10.9 %copy-start.1 = (bf16[64,2048]{1,0:T(8,128)(2,1)S(1)}, bf16[64,2048]{1,0:T(8,128)(2,1)}, u32[]{:S(2)}) copy-start(bf16[64,2048]{1,0:T(8,128)(2,1)} %param.11) | copy-start | bytes 786436
  27.3 3.2 copy-start.5
  32.2 3.8 %copy-start.2 = (bf16[32,704]{1,0:T(8,128)(2,1)S(1)}, bf16[32,704]{1,0:T(8,128)(2,1)}, u32[]{:S(2)}) copy-start(bf16[32,704]{1,0:T(8,128)(2,1)} %param.19) | copy-start | bytes 135172
  32.2 3.8 %copy-start.3 = (bf16[32,704]{1,0:T(8,128)(2,1)S(1)}, bf16[32,704]{1,0:T(8,128)(2,1)}, u32[]{:S(2)}) copy-start(bf16[32,704]{1,0:T(8,128)(2,1)} %param.20) | copy-start | bytes 135172
  32.2 3.8 %copy-start.4 = (bf16[704,32]{0,1:T(8,128)(2,1)S(1)}, bf16[704,32]{0,1:T(8,128)(2,1)}, u32[]{:S(2)}) copy-start(bf16[704,32]{0,1:T(8,128)(2,1)} %param.21) | copy-start | bytes 135172
  32.2 30.8 %all-to-all-start.1 = ((bf16[8,64,2048]{2,1,0:T(8,128)(2,1)}), bf16[8,64,2048]{2,1,0:T(8,128)(2,1)S(1)}, u32[]{:S(2)}, u32[]{:S(2)}) async-start(bf16[8,64,2048]{2,1,0:T(8,128)(2,1)} %broadcast_in_dim.16), calls=%async_computation.1 | async-start | bytes 4194304 | tf_op jit(solution)/shard_map/all_to_all | solution.py:43
  294.2 3.4 %copy-start = (bf16[64,32,2112]{2,1,0:T(8,128)(2,1)}, bf16[64,32,2112]{2,1,0:T(8,128)(2,1)S(1)}, u32[]{:S(2)}) copy-start(bf16[64,32,2112]{2,1,0:T(8,128)(2,1)S(1)} %all_to_all.35) | copy-start | bytes 25952260
